TPU v7x, 32 devices: a whole 2x2x4 slice. The times are simulated.
32 devices in a mesh: grp: 2 (over x), fs: 4 (over z), tp: 4 (over y, core).
Axes of the slice: x: 2, y: 2, z: 4, core: 2. Of those that a mesh axis runs over, the one named last changes fastest.
Arguments:
- tokens: bfloat16 [4096, 2048], P(('grp', 'fs')), parts along dimension 0, may hold values from -200 to 200
- norm_gain: float32 [2048], replicated, may hold values from 0.1 to 1.9
- value_weight: float32 [2048, 5632], P('fs', 'tp'), may hold values from -0.125 to 0.125
- gate_weight: float32 [2048, 5632], P('fs', 'tp'), may hold values from -0.125 to 0.125
- down_weight: float32 [2048, 5632], P('fs', 'tp'), may hold values from -0.078125 to 0.078125
- value_scale: float32 [5632], P('tp'), may hold values from 0.3 to 3
- gate_scale: float32 [5632], P('tp'), may hold values from 0.3 to 3
- down_scale: float32 [2048], replicated, may hold values from 0.3 to 3
- value_taps: float32 [3, 5632], P(None, 'tp'), may hold values from -3 to 3
- gate_taps: float32 [3, 5632], P(None, 'tp'), may hold values from -3 to 3
- value_bias: float32 [5632], P('tp'), may hold values from -3 to 3
- gate_bias: float32 [5632], P('tp'), may hold values from -3 to 3
Outputs:
- mixed: bfloat16 [4096, 2048], P(('grp', 'fs', 'tp')), parts along dimension 0
There are 2 independent parts, one for each index of `grp`. A program takes and returns all parts, laid end to end along the dimension named above; an argument that names none is the same for every part. Nothing has to cross between parts.
All inputs are finite; a program needn't handle non-finite values.
Results may differ from a plain program's by a relative error of at most 0.024.
Values may be sent and summed in bfloat16 or wider, within the bound.
A program may use at most 64 MiB of HBM per device.

v0:
```python
import jax
import jax.numpy as jnp
from jax import lax
from jax.sharding import PartitionSpec as P


def causal_mix(field, taps, bias):
    back_one = jnp.pad(field, ((1, 0), (0, 0)))[:-1]
    back_two = jnp.pad(field, ((2, 0), (0, 0)))[:-2]
    return taps[0] * back_two + taps[1] * back_one + taps[2] * field + bias


def local(
    tokens,
    norm_gain,
    value_weight,
    gate_weight,
    down_weight,
    value_scale,
    gate_scale,
    down_scale,
    value_taps,
    gate_taps,
    value_bias,
    gate_bias,
):
    floated = tokens.astype(jnp.float32)
    inverse = lax.rsqrt(jnp.mean(floated * floated, axis=-1, keepdims=True) + 1e-06)
    normed = (floated * inverse * norm_gain).astype(jnp.bfloat16)
    value_cast = value_weight.astype(jnp.bfloat16)
    gate_cast = gate_weight.astype(jnp.bfloat16)
    down_cast = down_weight.astype(jnp.bfloat16)
    value_full, gate_full, down_full = (
        lax.all_gather(value_cast, "fs", axis=0, tiled=True),
        lax.all_gather(gate_cast, "fs", axis=0, tiled=True),
        lax.all_gather(down_cast, "fs", axis=0, tiled=True),
    )
    value_up = jnp.dot(normed, value_full, preferred_element_type=jnp.float32)
    gate_up = jnp.dot(normed, gate_full, preferred_element_type=jnp.float32)
    value_mixed = causal_mix(value_up * value_scale, value_taps, value_bias)
    gate_mixed = causal_mix(gate_up * gate_scale, gate_taps, gate_bias)
    hidden = (jax.nn.silu(gate_mixed) * value_mixed).astype(jnp.bfloat16)
    total = lax.psum_scatter(
        lax.dot_general(
            hidden, down_full, (((1,), (1,)), ((), ())), preferred_element_type=jnp.float32
        ).astype(jnp.bfloat16),
        "tp",
        scatter_dimension=0,
        tiled=True,
    ).astype(jnp.float32)
    return (total * down_scale).astype(jnp.bfloat16)


def solution(mesh):
    return jax.shard_map(
        local,
        mesh=mesh,
        in_specs=(
            P(("grp", "fs"), None),
            P(),
            P("fs", "tp"),
            P("fs", "tp"),
            P("fs", "tp"),
            P("tp"),
            P("tp"),
            P(),
            P(None, "tp"),
            P(None, "tp"),
            P("tp"),
            P("tp"),
        ),
        out_specs=P(("grp", "fs", "tp"), None),
        check_vma=False,
    )
```

profile of v0, /device:TPU:0, one launch (start us, length us, event | category | flops | bytes accessed | tf_op | source)
XLA Modules:
  0.0 385.3 jit_solution(15212334096784148946)
XLA Ops:
  6.5 3.2 convert_element_type.36
  9.8 0.0 all-gather.6.cloned.1.call-update
  9.8 0.0 all-gather.4.cloned.1.call-start
  9.9 1.3 convert_element_type.35
  11.1 0.0 all-gather.4.cloned.1.call-update
  11.2 0.0 copy-start.2
  11.2 0.0 copy-start.3
  11.2 0.0 copy-start.1
  11.2 0.0 all-gather.8.cloned.1.call-start
  11.2 3.2 convert_element_type.38
  14.5 0.0 all-gather.8.cloned.1.call-update
  14.5 0.0 reduce-scatter.2.cloned.1.call-start
  14.6 0.1 slice_reduce_fusion.2
  14.7 0.5 fusion
  15.2 0.0 copy-start.7
  15.2 104.2 %all-gather.6.cloned.1.call-done = bf16[2048,1408]{1,0:T(8,128)(2,1)} async-done(((bf16[512,1408]{1,0:T(8,128)(2,1)}), bf16[2048,1408]{1,0:T(8,128)(2,1)}) %all-gather.6.cloned.1.call-update) | async-done | bytes 5767184 | tf_op jit(solution)/shard_map/all_gather | solution.py:34
  119.4 7.6 %convolution_multiply_fusion = f32[512,1408]{1,0:T(8,128)} fusion(bf16[2048,1408]{1,0:T(8,128)(2,1)} %all-gather.6.cloned.1.call-done, f32[1408]{0:T(1024)S(1)} %copy-done.5, bf16[512,2048]{1,0:T(8,128)(2,1)S(1)} %copy-done.1, f32[2048]{0:T(1024)S(1)} %copy-done.6, f32[512]{0:T(512)S(1)} %add_rsqrt_fusion), kind=kOutput, calls=%fused_computation.5 | convolution fusion | flops 2957705216 | bytes 10763776 | tf_op jit(solution)/shard_map/dot_general | solution.py:38
  127.0 98.9 %all-gather.4.cloned.1.call-done = bf16[2048,1408]{1,0:T(8,128)(2,1)} async-done(((bf16[512,1408]{1,0:T(8,128)(2,1)}), bf16[2048,1408]{1,0:T(8,128)(2,1)}) %all-gather.4.cloned.1.call-update) | async-done | bytes 5767184 | tf_op jit(solution)/shard_map/all_gather | solution.py:35
  225.9 7.7 %convolution_multiply_fusion.1 = f32[512,1408]{1,0:T(8,128)} fusion(bf16[2048,1408]{1,0:T(8,128)(2,1)} %all-gather.4.cloned.1.call-done, f32[1408]{0:T(1024)S(1)} %copy-done.7, bf16[512,2048]{1,0:T(8,128)(2,1)S(1)} %copy-done.1, f32[2048]{0:T(1024)S(1)} %copy-done.6, f32[512]{0:T(512)S(1)} %add_rsqrt_fusion), kind=kOutput, calls=%fused_computation.6 | convolution fusion | flops 2957705216 | bytes 10763776 | tf_op jit(solution)/shard_map/dot_general | solution.py:39
  233.7 98.8 %all-gather.8.cloned.1.call-done = bf16[2048,1408]{1,0:T(8,128)(2,1)} async-done(((bf16[512,1408]{1,0:T(8,128)(2,1)}), bf16[2048,1408]{1,0:T(8,128)(2,1)}) %all-gather.8.cloned.1.call-update) | async-done | bytes 5767184 | tf_op jit(solution)/shard_map/all_gather | solution.py:36
  332.5 14.7 %convolution_convert_fusion = bf16[512,2048]{1,0:T(8,128)(2,1)} fusion(bf16[2048,1408]{1,0:T(8,128)(2,1)} %all-gather.8.cloned.1.call-done, f32[512,1408]{1,0:T(8,128)} %convolution_multiply_fusion, f32[512,1408]{1,0:T(8,128)} %convolution_multiply_fusion.1, f32[1408]{0:T(1024)S(1)} %copy-done.8, f32[1408]{0:T(1024)S(1)} %get-tuple-element.9, ...), kind=kOutput, calls=%fused_computation.7 | convolution fusion | flops 2966814720 | bytes 13676544 | tf_op jit(solution)/shard_map/dot_general | solution.py:44
  347.2 0.0 reduce-scatter.2.cloned.1.call-update
  347.2 29.6 %reduce-scatter.2.cloned.1.call-done = bf16[128,2048]{1,0:T(8,128)(2,1)} async-done(((bf16[512,2048]{1,0:T(8,128)(2,1)}), bf16[128,2048]{1,0:T(8,128)(2,1)}) %reduce-scatter.2.cloned.1.call-update) | async-done | bytes 524304 | tf_op jit(solution)/shard_map/reduce_scatter | solution.py:43
  376.8 1.9 multiply_convert_fusion
  (18 shorter events, 0.0 us)
Async XLA Ops:
  6.5 3.3 copy-start
  6.5 112.8 %all-gather.6.cloned.1.call-start = ((), (), s32[]{:S(2)}) async-start(), calls=%async_computation.2 | async-start | bytes 7208960 | tf_op jit(solution)/shard_map/all_gather | solution.py:34
  9.8 216.1 %all-gather.4.cloned.1.call-start = ((), (), s32[]{:S(2)}) async-start(), calls=%async_computation.1 | async-start | bytes 7208960 | tf_op jit(solution)/shard_map/all_gather | solution.py:35
  11.2 3.4 copy-start.2
  11.2 3.4 copy-start.3
  11.2 3.5 copy-start.1
  11.2 321.3 %all-gather.8.cloned.1.call-start = ((), (), s32[]{:S(2)}) async-start(), calls=%async_computation.3 | async-start | bytes 7208960 | tf_op jit(solution)/shard_map/all_gather | solution.py:36
  14.5 104.9 %copy-start.5 = (f32[1408]{0:T(1024)S(1)}, f32[1408]{0:T(1024)}, u32[]{:S(2)}) copy-start(f32[1408]{0:T(1024)} %param.17) | copy-start | bytes 16900
  14.5 104.9 %copy-start.6 = (f32[2048]{0:T(1024)S(1)}, f32[2048]{0:T(1024)}, u32[]{:S(2)}) copy-start(f32[2048]{0:T(1024)} %param.13) | copy-start | bytes 24580
  14.5 362.3 %reduce-scatter.2.cloned.1.call-start = ((), (), s32[]{:S(2)}) async-start(), calls=%async_computation.4 | async-start | bytes 2621440 | tf_op jit(solution)/shard_map/reduce_scatter | solution.py:43
  15.2 210.7 %copy-start.7 = (f32[1408]{0:T(1024)S(1)}, f32[1408]{0:T(1024)}, u32[]{:S(2)}) copy-start(f32[1408]{0:T(1024)} %param.18) | copy-start | bytes 16900
  127.0 205.5 %copy-start.8 = (f32[1408]{0:T(1024)S(1)}, f32[1408]{0:T(1024)}, u32[]{:S(2)}) copy-start(f32[1408]{0:T(1024)} %param.22) | copy-start | bytes 16900
  127.0 205.5 %copy-start.9 = (f32[1408]{0:T(1024)S(1)}, f32[1408]{0:T(1024)}, u32[]{:S(2)}) copy-start(f32[1408]{0:T(1024)} %param.23) | copy-start | bytes 16900
  332.5 44.3 %copy-start.4 = (f32[2048]{0:T(1024)S(1)}, f32[2048]{0:T(1024)}, u32[]{:S(2)}) copy-start(f32[2048]{0:T(1024)} %param.19) | copy-start | bytes 24580
Sparse Core Ops, SparseCore 0:
  9.9 109.3 all-gather.5
  120.9 104.9 all-gather.3
  227.5 104.9 all-gather.7
  347.3 29.4 reduce-scatter.1
where the time goes:
time: 385 us
  waiting for transfers between devices  332 us (86%)
  matrix products  30.1 us (8%)
  between operations  13.2 us (3%)
  other arithmetic  10.2 us (3%)
    all_gather x1, waiting for transfers between devices, local(): lax.all_gather(value_cast, 'fs', axis=0, tiled=True)  104 us
    all_gather x1, waiting for transfers between devices, local(): lax.all_gather(gate_cast, 'fs', axis=0, tiled=True)  98.9 us
    all_gather x1, waiting for transfers between devices, local(): lax.all_gather(down_cast, 'fs', axis=0, tiled=True)  98.8 us
    reduce_scatter x1, waiting for transfers between devices, local(): lax.psum_scatter(lax.dot_general(hidden, down_full, (((1,), (1,)), ((), (...  29.6 us
    dot_general x1, matrix products, local(): lax.dot_general(hidden, down_full, (((1,), (1,)), ((), ())), preferred_el...  14.7 us
    dot_general x1, matrix products, local(): gate_up = jnp.dot(normed, gate_full, preferred_element_type=jnp.float32)  7.74 us
  transfers between devices with their start and end apart: 4, of which 4 were waited for; matrix products, arithmetic and copies ran while one was open for 5% of the time, Pallas kernels for 0%

commit v1 on v0

v1 whole, which is shorter than its diff:
```python
import functools

import jax
import jax.numpy as jnp
from jax import lax
from jax.experimental import pallas as pl
from jax.experimental.pallas import tpu as pltpu
from jax.sharding import PartitionSpec as P

MESH = pl.DeviceIdType.MESH
WIDE = 256
RIGHT, LEFT, ACROSS = 0, 1, 2


def kernel(
    parts,
    line,
    peers,
    pieces,
    tokens,
    norm_gain,
    value_weight,
    gate_weight,
    down_weight,
    value_scale,
    gate_scale,
    down_scale,
    value_taps,
    gate_taps,
    value_bias,
    gate_bias,
    out,
    value_full,
    gate_full,
    down_full,
    normed,
    mixed,
    hidden,
    partial,
    landed,
    send_sem,
    recv_sem,
    sum_send,
    sum_recv,
):
    group, here, me = lax.axis_index("grp"), lax.axis_index("fs"), lax.axis_index("tp")
    full = (value_full, gate_full, down_full)
    shards = (value_weight, gate_weight, down_weight)
    rows, units = hidden.shape
    held = shards[0].shape[0]
    share = held // parts
    piece = share // pieces
    kept = rows // peers

    def greet(act):
        pl.when(here > 0)(lambda: act("fs", here - 1))
        pl.when(here < line - 1)(lambda: act("fs", here + 1))
        for k in range(1, parts):
            act("grp", lax.rem(group + k, parts))
        for k in range(1, peers):
            act("tp", lax.rem(me + k, peers))

    barrier = pltpu.get_barrier_semaphore()
    greet(
        lambda axis, index: pl.semaphore_signal(
            barrier, inc=1, device_id={axis: index}, device_id_type=MESH
        )
    )

    def cast(which):
        step = min(held, 64)

        def body(i, carry):
            source = pl.ds(pl.multiple_of(i * step, step), step)
            target = pl.ds(pl.multiple_of(here * held + i * step, step), step)
            full[which][target, :] = shards[which][source, :].astype(jnp.bfloat16)
            return carry

        lax.fori_loop(0, held // step, body, 0)

    def copy(which, owner, part, slot, direction):
        first = pl.multiple_of(owner * held + part * share + slot * piece, piece)
        block = full[which].at[pl.ds(first, piece), :]
        if direction == RIGHT:
            target = {"fs": lax.min(here + 1, line - 1)}
        elif direction == LEFT:
            target = {"fs": lax.max(here - 1, 0)}
        else:
            target = {"grp": lax.rem(group + direction - ACROSS + 1, parts)}
        return pltpu.make_async_remote_copy(
            src_ref=block,
            dst_ref=block,
            send_sem=send_sem.at[which, owner, slot, direction],
            recv_sem=recv_sem.at[which, owner, part, slot],
            device_id=target,
            device_id_type=MESH,
        )

    def own(which, act):
        for slot in range(pieces):
            pl.when(here < line - 1)(lambda: act(copy(which, here, group, slot, RIGHT)))
            pl.when(here > 0)(lambda: act(copy(which, here, group, slot, LEFT)))

    def onward(which, step, act, arrive):
        for slot in range(pieces):
            for direction in (RIGHT, LEFT):
                owner = here - step if direction == RIGHT else here + step
                there = owner >= 0 if direction == RIGHT else owner < line
                more = here < line - 1 if direction == RIGHT else here > 0

                @pl.when(there)
                def _():
                    if arrive:
                        copy(which, owner, group, slot, direction).wait_recv()
                    pl.when(more)(lambda: act(copy(which, owner, group, slot, direction)))
                    for k in range(parts - 1):
                        act(copy(which, owner, group, slot, ACROSS + k))

    def crossed(which, step):
        for slot in range(pieces):
            for owner, there in ((here - step, here >= step), (here + step, here + step < line)):

                @pl.when(there)
                def _():
                    for k in range(parts - 1):
                        part = lax.rem(group + k + 1, parts)
                        copy(which, owner, part, slot, ACROSS + k).wait_recv()

    def start(dma):
        dma.start()

    def left(dma):
        dma.wait_send()

    def normalize():
        step = min(rows, 64)

        def body(i, carry):
            block = pl.ds(pl.multiple_of(i * step, step), step)
            floated = tokens[block, :].astype(jnp.float32)
            mean = jnp.mean(floated * floated, axis=-1, keepdims=True)
            normed[block, :] = (floated * lax.rsqrt(mean + 1e-06) * norm_gain[...]).astype(
                jnp.bfloat16
            )
            return carry

        lax.fori_loop(0, rows // step, body, 0)

    def over_units(body):
        if units // WIDE:

            def one(i, carry):
                body(pl.ds(pl.multiple_of(i * WIDE, WIDE), WIDE), WIDE)
                return carry

            lax.fori_loop(0, units // WIDE, one, 0)
        if units % WIDE:
            body(pl.ds(units // WIDE * WIDE, units % WIDE), units % WIDE)

    def causal(which, scale, taps, bias, columns, width):
        up = jnp.dot(normed[...], full[which][:, columns], preferred_element_type=jnp.float32)
        up = up * scale[:, columns]
        position = lax.broadcasted_iota(jnp.int32, (rows, width), 0)
        one = jnp.where(position >= 1, pltpu.roll(up, 1, axis=0), 0.0)
        two = jnp.where(position >= 2, pltpu.roll(up, 2, axis=0), 0.0)
        return (
            taps[0:1, columns] * two
            + taps[1:2, columns] * one
            + taps[2:3, columns] * up
            + bias[:, columns]
        )

    def value(columns, width):
        mixed[:, columns] = causal(0, value_scale, value_taps, value_bias, columns, width)

    def gate(columns, width):
        gated = causal(1, gate_scale, gate_taps, gate_bias, columns, width)
        hidden[:, columns] = (gated / (1.0 + jnp.exp(-gated)) * mixed[:, columns]).astype(
            jnp.bfloat16
        )

    def give(owner, k):
        peer = lax.rem(me + k, peers)
        return pltpu.make_async_remote_copy(
            src_ref=partial.at[owner, pl.ds(pl.multiple_of(peer * kept, kept), kept), :],
            dst_ref=landed.at[k - 1, owner],
            send_sem=sum_send,
            recv_sem=sum_recv,
            device_id={"tp": peer},
            device_id_type=MESH,
        )

    def project(owner):
        block = full[2][pl.ds(pl.multiple_of(owner * held, held), held), :]
        partial[owner] = lax.dot_general(
            hidden[...], block, (((1,), (1,)), ((), ())), preferred_element_type=jnp.float32
        ).astype(jnp.bfloat16)
        for k in range(1, peers):
            give(owner, k).start()

    def project_at(step):
        crossed(2, step)
        pl.when(here >= step)(lambda: project(here - step))
        pl.when(here + step < line)(lambda: project(here + step))

    cast(0)
    ends = (here == 0).astype(jnp.int32) + (here == line - 1).astype(jnp.int32)
    pl.semaphore_wait(barrier, parts + peers - ends)
    own(0, start)
    cast(1)
    own(1, start)
    cast(2)
    normalize()
    for step in range(1, line):
        onward(0, step, start, True)
    onward(1, 1, start, True)
    own(2, start)
    for step in range(1, line):
        crossed(0, step)
    over_units(value)
    for step in range(2, line):
        onward(1, step, start, True)
    onward(2, 1, start, True)
    for step in range(1, line):
        crossed(1, step)
    over_units(gate)
    project(here)
    for step in range(2, line):
        onward(2, step, start, True)
        project_at(step - 1)
    project_at(line - 1)

    pltpu.make_async_copy(landed, landed, sum_recv).wait()
    mine = pl.ds(pl.multiple_of(me * kept, kept), kept)
    for owner in range(line):
        total = partial[owner, mine, :].astype(jnp.float32)
        for k in range(peers - 1):
            total = total + landed[k, owner].astype(jnp.float32)
        columns = slice(owner * held, (owner + 1) * held)
        out[:, columns] = (total * down_scale[:, columns]).astype(jnp.bfloat16)

    pltpu.make_async_copy(landed, landed, sum_send).wait()
    for which in range(3):
        own(which, left)
        for step in range(1, line):
            onward(which, step, left, False)


def solution(mesh):
    parts, line, peers = mesh.shape["grp"], mesh.shape["fs"], mesh.shape["tp"]

    def local(tokens, norm_gain, *rest):
        weights, scales, taps, biases = rest[:3], rest[3:6], rest[6:8], rest[8:]
        rows, width = tokens.shape
        held, units = weights[0].shape
        share = held // parts
        pieces = 2 if share % 2 == 0 and share // 2 >= 128 else 1
        kept = rows // peers
        whole = [pltpu.VMEM((width, units), jnp.bfloat16)] * 3
        return pl.pallas_call(
            functools.partial(kernel, parts, line, peers, pieces),
            out_shape=jax.ShapeDtypeStruct((kept, width), jnp.bfloat16),
            in_specs=[pl.BlockSpec(memory_space=pltpu.VMEM)] * 12,
            out_specs=pl.BlockSpec(memory_space=pltpu.VMEM),
            scratch_shapes=whole
            + [
                pltpu.VMEM((rows, width), jnp.bfloat16),
                pltpu.VMEM((rows, units), jnp.float32),
                pltpu.VMEM((rows, units), jnp.bfloat16),
                pltpu.VMEM((line, rows, held), jnp.bfloat16),
                pltpu.VMEM((peers - 1, line, kept, held), jnp.bfloat16),
                pltpu.SemaphoreType.DMA((3, line, pieces, 1 + parts)),
                pltpu.SemaphoreType.DMA((3, line, parts, pieces)),
                pltpu.SemaphoreType.DMA,
                pltpu.SemaphoreType.DMA,
            ],
            compiler_params=pltpu.CompilerParams(
                collective_id=0, has_side_effects=True, vmem_limit_bytes=60 * 1024 * 1024
            ),
        )(
            tokens,
            norm_gain[None],
            *weights,
            *(scale[None] for scale in scales),
            *taps,
            *(bias[None] for bias in biases),
        )

    return jax.shard_map(
        local,
        mesh=mesh,
        in_specs=(
            P(("grp", "fs"), None),
            P(),
            P("fs", "tp"),
            P("fs", "tp"),
            P("fs", "tp"),
            P("tp"),
            P("tp"),
            P(),
            P(None, "tp"),
            P(None, "tp"),
            P("tp"),
            P("tp"),
        ),
        out_specs=P(("grp", "fs", "tp"), None),
        check_vma=False,
    )
```

time: 385 us -> 189 us (0.49)
  waiting for transfers between devices: 332 us -> 0 us
  Pallas kernels: 0 us -> 181 us
  matrix products: 30.1 us -> 0 us
  between operations: 13.2 us -> 0.01 us
  other arithmetic: 10.2 us -> 0 us
  local copies, waits for them, and re-layouts: 0.14 us -> 7.05 us
    all_gather x3 -> x0, waiting for transfers between devices: 302 us -> none  [the longest x1 104 us: local(): lax.all_gather(value_cast, 'fs', axis=0, tiled=True)]
    pallas_call x0 -> x1, Pallas kernels: none -> 181 us  [local(): pl.pallas_call(functools.partial(kernel, parts, line, peers, pieces), out...]
    dot_general x3 -> x0, matrix products: 30.1 us -> none  [the longest x1 14.7 us: local(): lax.dot_general(hidden, down_full, (((1,), (1,)), ((), ())), preferred_el...]
    reduce_scatter x1 -> x0, waiting for transfers between devices: 29.6 us -> none  [local(): lax.psum_scatter(lax.dot_general(hidden, down_full, (((1,), (1,)), ((), (...]
    convert_element_type x4 -> x0, other arithmetic: 9.67 us -> none  [the longest x1 3.23 us: local(): value_cast = value_weight.astype(jnp.bfloat16)]
    broadcast_in_dim x0 -> x4, local copies, waits for them, and re-layouts: none -> 5.17 us  [the longest x2 2.59 us: local(): scale[None]]
  transfers between devices with their start and end apart: 4 -> 0, of which waited for: 4 -> 0; matrix products, arithmetic and copies ran while one was open for 5% -> 0% of each run, Pallas kernels for 0% -> 0%
where the time goes in v1:
time: 189 us; the launch traced here: 188 us
  Pallas kernels  181 us (96%)
  local copies, waits for them, and re-layouts  7.05 us (4%)
    pallas_call x1, Pallas kernels, local(): pl.pallas_call(functools.partial(kernel, parts, line, peers, pieces), out...  181 us

profile of v1, /device:TPU:0, one launch (start us, length us, event | category | flops | bytes accessed | tf_op | source)
XLA Modules:
  0.0 188.1 jit_solution(4623609000474017511)
XLA Ops:
  0.0 1.3 broadcast_in_dim.19.value_scale
  1.3 1.3 broadcast_in_dim.20.gate_scale
  2.6 1.3 broadcast_in_dim.22.value_bias
  3.9 1.3 broadcast_in_dim.23.gate_bias
  5.2 181.0 %shard_map.118 = bf16[128,2048]{1,0:T(8,128)(2,1)} custom-call(bf16[512,2048]{1,0:T(8,128)(2,1)} %tokens.1, f32[1,2048]{1,0:T(1,128)} %bitcast.2, f32[512,1408]{1,0:T(8,128)} %value_weight.1, f32[512,1408]{1,0:T(8,128)} %gate_weight.1, f32[512,1408]{1,0:T(8,128)} %down_weight.1, f32[1,1408]{1,0:T(1,128)} %broadcast_in_dim.19.value_scale, ...), custom_call_target="tpu_custom_call" | custom-call | tf_op jit(solution)/shard_map/pallas_call | solution.py:260
  186.2 1.9 %copy.14 = bf16[128,2048]{1,0:T(8,128)(2,1)} copy(bf16[128,2048]{1,0:T(8,128)(2,1)} %shard_map.118) | data formatting | bytes 1048576

commit v2 on v1

v2 whole, which is shorter than its diff:
```python
import functools

import jax
import jax.numpy as jnp
from jax import lax
from jax.experimental import pallas as pl
from jax.experimental.pallas import tpu as pltpu
from jax.sharding import PartitionSpec as P

MESH = pl.DeviceIdType.MESH
WIDE = 256
RIGHT, LEFT, ACROSS = 0, 1, 2


def kernel(
    parts,
    line,
    peers,
    pieces,
    lent,
    tokens,
    norm_gain,
    value_weight,
    gate_weight,
    down_weight,
    value_scale,
    gate_scale,
    down_scale,
    value_taps,
    gate_taps,
    value_bias,
    gate_bias,
    out,
    *scratch,
):
    group, here, me = lax.axis_index("grp"), lax.axis_index("fs"), lax.axis_index("tp")
    scratch = list(scratch)
    take = lambda count: [scratch.pop(0) for _ in range(count)]
    kinds = 2 if lent else 1
    full = take(3 * kinds)
    normed, partial, landed, along, wide = take(5)
    mixed, hidden = take(kinds), take(kinds)
    send_sem, recv_sem, sum_send, sum_recv = take(4)
    if lent:
        guest, guest_mixed, guest_hidden, guest_partial, guest_landed, summed, returned = take(7)
        lend_send, lend_recv, guest_send, guest_recv = take(4)
        back_send, back_recv = take(2)
    shards = (value_weight, gate_weight, down_weight)
    rows = tokens.shape[0]
    held, units = shards[0].shape
    share = held // parts
    piece = share // pieces
    kept = rows // peers
    base = (0, units - lent)
    span = (units - lent, lent)
    end = jnp.logical_or(here == 0, here == line - 1)
    inner = jnp.logical_not(end)
    helper = jnp.logical_and(inner, jnp.logical_or(here == 1, here == line - 2))
    mate = jnp.where(end, jnp.where(here == 0, 1, line - 2), jnp.where(here == 1, 0, line - 1))

    barrier = pltpu.get_barrier_semaphore()

    def greet(axis, index):
        pl.semaphore_signal(barrier, inc=1, device_id={axis: index}, device_id_type=MESH)

    pl.when(here > 0)(lambda: greet("fs", here - 1))
    pl.when(here < line - 1)(lambda: greet("fs", here + 1))
    for k in range(1, parts):
        greet("grp", lax.rem(group + k, parts))
    for k in range(1, peers):
        greet("tp", lax.rem(me + k, peers))

    def spread():
        for i, vector in enumerate((value_scale, gate_scale, value_bias, gate_bias)):
            along[i : i + 1, :] = vector[...].reshape(1, units)
        for i, vector in enumerate((norm_gain, down_scale)):
            wide[i : i + 1, :] = vector[...].reshape(1, vector.shape[0])

    def cast(which):
        step = min(held, 64)

        def body(i, carry):
            source = pl.ds(pl.multiple_of(i * step, step), step)
            target = pl.ds(pl.multiple_of(here * held + i * step, step), step)
            for kind in range(kinds):
                columns = slice(base[kind], base[kind] + span[kind])
                full[which + 3 * kind][target, :] = shards[which][source, columns].astype(
                    jnp.bfloat16
                )
            return carry

        lax.fori_loop(0, held // step, body, 0)

    def copy(which, owner, part, slot, direction):
        first = pl.multiple_of(owner * held + part * share + slot * piece, piece)
        block = full[which].at[pl.ds(first, piece), :]
        if direction == RIGHT:
            target = {"fs": lax.min(here + 1, line - 1)}
        elif direction == LEFT:
            target = {"fs": lax.max(here - 1, 0)}
        else:
            target = {"grp": lax.rem(group + direction - ACROSS + 1, parts)}
        return pltpu.make_async_remote_copy(
            src_ref=block,
            dst_ref=block,
            send_sem=send_sem.at[which, owner, slot, direction],
            recv_sem=recv_sem.at[which, owner, part, slot],
            device_id=target,
            device_id_type=MESH,
        )

    def more(which, direction):
        edge = 0 if which < 3 else 1
        return here < line - 1 - edge if direction == RIGHT else here > edge

    def comes(which, owner):
        inside = jnp.logical_and(owner >= 0, owner < line)
        return inside if which < 3 else jnp.logical_and(inside, inner)

    def own(which, act):
        for each in range(which, 3 * kinds, 3):
            for slot in range(pieces):
                for direction in (RIGHT, LEFT):
                    pl.when(more(each, direction))(
                        lambda: act(copy(each, here, group, slot, direction))
                    )

    def onward(which, step, act, arrive):
        for each in range(which, 3 * kinds, 3):
            for slot in range(pieces):
                for direction in (RIGHT, LEFT):
                    owner = here - step if direction == RIGHT else here + step

                    @pl.when(comes(each, owner))
                    def _():
                        if arrive:
                            copy(each, owner, group, slot, direction).wait_recv()
                        pl.when(more(each, direction))(
                            lambda: act(copy(each, owner, group, slot, direction))
                        )
                        for k in range(parts - 1):
                            act(copy(each, owner, group, slot, ACROSS + k))

    def crossed(which, step):
        for each in range(which, 3 * kinds, 3):
            for slot in range(pieces):
                for owner in (here - step, here + step):

                    @pl.when(comes(each, owner))
                    def _():
                        for k in range(parts - 1):
                            part = lax.rem(group + k + 1, parts)
                            copy(each, owner, part, slot, ACROSS + k).wait_recv()

    def start(dma):
        dma.start()

    def left(dma):
        dma.wait_send()

    def normalize(source, offset):
        step = min(rows, 64)

        def body(i, carry):
            block = pl.ds(pl.multiple_of(i * step, step), step)
            target = pl.ds(pl.multiple_of(offset + i * step, step), step)
            floated = source[block, :].astype(jnp.float32)
            mean = jnp.mean(floated * floated, axis=-1, keepdims=True)
            normed[target, :] = (floated * lax.rsqrt(mean + 1e-06) * wide[0:1, :]).astype(
                jnp.bfloat16
            )
            return carry

        lax.fori_loop(0, rows // step, body, 0)

    mine = pl.ds(pl.multiple_of(me * kept, kept), kept)

    def lend():
        return pltpu.make_async_remote_copy(
            src_ref=tokens.at[mine, :],
            dst_ref=guest.at[mine, :],
            send_sem=lend_send,
            recv_sem=lend_recv,
            device_id={"fs": mate},
            device_id_type=MESH,
        )

    def relay(k):
        return pltpu.make_async_remote_copy(
            src_ref=guest.at[mine, :],
            dst_ref=guest.at[mine, :],
            send_sem=guest_send.at[line],
            recv_sem=guest_recv.at[line],
            device_id={"tp": lax.rem(me + k, peers)},
            device_id_type=MESH,
        )

    def relays():
        lend().wait_recv()
        for k in range(1, peers):
            relay(k).start()

    def guest_rows():
        others = guest.at[pl.ds(0, (peers - 1) * kept), :]
        return others

    def welcome():
        pltpu.make_async_copy(guest_rows(), guest_rows(), guest_recv.at[line]).wait()
        normalize(guest, rows)

    def over_units(kind, body):
        count = span[kind]
        if count // WIDE:

            def one(i, carry):
                first = pl.multiple_of(i * WIDE, WIDE)
                shifted = pl.multiple_of(base[kind] + i * WIDE, 128)
                body(pl.ds(first, WIDE), pl.ds(shifted, WIDE), WIDE)
                return carry

            lax.fori_loop(0, count // WIDE, one, 0)
        if count % WIDE:
            first = count // WIDE * WIDE
            body(pl.ds(first, count % WIDE), pl.ds(base[kind] + first, count % WIDE), count % WIDE)

    def causal(which, branch, taps, offset, columns, outer, width):
        up = jnp.dot(
            normed[offset : offset + rows, :],
            full[which][:, columns],
            preferred_element_type=jnp.float32,
        )
        up = up * along[branch : branch + 1, outer]
        position = lax.broadcasted_iota(jnp.int32, (rows, width), 0)
        one = jnp.where(position >= 1, pltpu.roll(up, 1, axis=0), 0.0)
        two = jnp.where(position >= 2, pltpu.roll(up, 2, axis=0), 0.0)
        return (
            taps[0:1, outer] * two
            + taps[1:2, outer] * one
            + taps[2:3, outer] * up
            + along[branch + 2 : branch + 3, outer]
        )

    def value(kind, keep, offset):
        def body(columns, outer, width):
            keep[:, columns] = causal(
                3 * kind, 0, value_taps, offset, columns, outer, width
            )

        over_units(kind, body)

    def gate(kind, kept_value, keep, offset):
        def body(columns, outer, width):
            gated = causal(1 + 3 * kind, 1, gate_taps, offset, columns, outer, width)
            keep[:, columns] = (
                gated / (1.0 + jnp.exp(-gated)) * kept_value[:, columns]
            ).astype(jnp.bfloat16)

        over_units(kind, body)

    def give(owner, k):
        peer = lax.rem(me + k, peers)
        return pltpu.make_async_remote_copy(
            src_ref=partial.at[owner, pl.ds(pl.multiple_of(peer * kept, kept), kept), :],
            dst_ref=landed.at[k - 1, owner],
            send_sem=sum_send,
            recv_sem=sum_recv,
            device_id={"tp": peer},
            device_id_type=MESH,
        )

    def guest_give(owner, k):
        peer = lax.rem(me + k, peers)
        return pltpu.make_async_remote_copy(
            src_ref=guest_partial.at[owner, pl.ds(pl.multiple_of(peer * kept, kept), kept), :],
            dst_ref=guest_landed.at[owner, k - 1],
            send_sem=guest_send.at[owner],
            recv_sem=guest_recv.at[owner],
            device_id={"tp": peer},
            device_id_type=MESH,
        )

    def down(left_side, kind, owner):
        block = full[2 + 3 * kind][pl.ds(pl.multiple_of(owner * held, held), held), :]
        return lax.dot_general(
            left_side[...], block, (((1,), (1,)), ((), ())), preferred_element_type=jnp.float32
        )

    def project(owner):
        if not lent:
            partial[owner] = down(hidden[0], 0, owner).astype(jnp.bfloat16)
        else:

            @pl.when(helper)
            def _():
                guest_partial[owner] = down(guest_hidden, 1, owner).astype(jnp.bfloat16)
                for k in range(1, peers):
                    guest_give(owner, k).start()

            @pl.when(inner)
            def _():
                partial[owner] = (down(hidden[0], 0, owner) + down(hidden[1], 1, owner)).astype(
                    jnp.bfloat16
                )

            @pl.when(end)
            def _():
                partial[owner] = down(hidden[0], 0, owner).astype(jnp.bfloat16)

        for k in range(1, peers):
            give(owner, k).start()

    def back(owner):
        return pltpu.make_async_remote_copy(
            src_ref=summed.at[owner],
            dst_ref=returned.at[owner],
            send_sem=back_send,
            recv_sem=back_recv,
            device_id={"fs": mate},
            device_id_type=MESH,
        )

    def give_back(owner):
        if lent:

            @pl.when(helper)
            def _():
                arrived = guest_landed.at[owner]
                pltpu.make_async_copy(arrived, arrived, guest_recv.at[owner]).wait()
                total = guest_partial[owner, mine, :].astype(jnp.float32)
                for k in range(peers - 1):
                    total = total + guest_landed[owner, k].astype(jnp.float32)
                summed[owner] = total.astype(jnp.bfloat16)
                back(owner).start()

    def around(step, act):
        pl.when(here >= step)(lambda: act(here - step))
        pl.when(here + step < line)(lambda: act(here + step))

    def project_at(step):
        crossed(2, step)
        around(step, project)

    spread()
    cast(0)
    ends = (here == 0).astype(jnp.int32) + (here == line - 1).astype(jnp.int32)
    pl.semaphore_wait(barrier, parts + peers - ends)
    own(0, start)
    if lent:
        pl.when(end)(lambda: lend().start())
    cast(1)
    own(1, start)
    cast(2)
    normalize(tokens, 0)
    for step in range(1, line):
        onward(0, step, start, True)
        if lent and step == 1:
            pl.when(helper)(relays)
    onward(1, 1, start, True)
    own(2, start)
    for step in range(1, line):
        crossed(0, step)
    value(0, mixed[0], 0)
    if lent:
        pl.when(inner)(lambda: value(1, mixed[1], 0))

        @pl.when(helper)
        def _():
            welcome()
            value(1, guest_mixed, rows)

    for step in range(2, line):
        onward(1, step, start, True)
    onward(2, 1, start, True)
    for step in range(1, line):
        crossed(1, step)
    gate(0, mixed[0], hidden[0], 0)
    if lent:
        pl.when(inner)(lambda: gate(1, mixed[1], hidden[1], 0))
        pl.when(helper)(lambda: gate(1, guest_mixed, guest_hidden, rows))
    project(here)
    for step in range(2, line):
        onward(2, step, start, True)
        project_at(step - 1)
        if step == 2:
            give_back(here)
        else:
            around(step - 2, give_back)
    project_at(line - 1)
    for step in range(max(line - 2, 1), line):
        around(step, give_back)

    pltpu.make_async_copy(landed, landed, sum_recv).wait()

    def finish(extra):
        for owner in range(line):
            total = partial[owner, mine, :].astype(jnp.float32)
            for k in range(peers - 1):
                total = total + landed[k, owner].astype(jnp.float32)
            if extra:
                total = total + returned[owner].astype(jnp.float32)
            columns = slice(owner * held, (owner + 1) * held)
            out[:, columns] = (total * wide[1:2, columns]).astype(jnp.bfloat16)

    if lent:

        @pl.when(end)
        def _():
            pltpu.make_async_copy(returned, returned, back_recv).wait()
            finish(True)
            lend().wait_send()

        pl.when(inner)(lambda: finish(False))

        @pl.when(helper)
        def _():
            pltpu.make_async_copy(guest_rows(), guest_rows(), guest_send.at[line]).wait()
            for owner in range(line):
                sent = guest_landed.at[owner]
                pltpu.make_async_copy(sent, sent, guest_send.at[owner]).wait()
            pltpu.make_async_copy(summed, summed, back_send).wait()

    else:
        finish(False)

    pltpu.make_async_copy(landed, landed, sum_send).wait()
    for which in range(3):
        own(which, left)
        for step in range(1, line):
            onward(which, step, left, False)


def solution(mesh):
    parts, line, peers = mesh.shape["grp"], mesh.shape["fs"], mesh.shape["tp"]

    def local(*arrays):
        rows, width = arrays[0].shape
        held, units = arrays[2].shape
        share = held // parts
        pieces = 2 if share % 2 == 0 and share // 2 >= 128 else 1
        kept = rows // peers
        lent = units * 5 // 11 // 128 * 128 if line >= 4 and peers > 1 else 0
        half, full = jnp.bfloat16, jnp.float32
        spans = (units - lent, lent) if lent else (units,)
        dma = pltpu.SemaphoreType.DMA
        scratch = [pltpu.VMEM((width, span), half) for span in spans for _ in range(3)]
        scratch += [
            pltpu.VMEM((rows * len(spans), width), half),
            pltpu.VMEM((line, rows, held), half),
            pltpu.VMEM((peers - 1, line, kept, held), half),
            pltpu.VMEM((4, units), full),
            pltpu.VMEM((2, width), full),
        ]
        scratch += [pltpu.VMEM((rows, span), full) for span in spans]
        scratch += [pltpu.VMEM((rows, span), half) for span in spans]
        scratch += [
            dma((3 * len(spans), line, pieces, 1 + parts)),
            dma((3 * len(spans), line, parts, pieces)),
            dma,
            dma,
        ]
        if lent:
            scratch += [
                pltpu.VMEM((rows, width), half),
                pltpu.VMEM((rows, lent), full),
                pltpu.VMEM((rows, lent), half),
                pltpu.VMEM((line, rows, held), half),
                pltpu.VMEM((line, peers - 1, kept, held), half),
                pltpu.VMEM((line, kept, held), half),
                pltpu.VMEM((line, kept, held), half),
                dma,
                dma,
                dma((line + 1,)),
                dma((line + 1,)),
                dma,
                dma,
            ]
        return pl.pallas_call(
            functools.partial(kernel, parts, line, peers, pieces, lent),
            out_shape=jax.ShapeDtypeStruct((kept, width), half),
            in_specs=[pl.BlockSpec(memory_space=pltpu.VMEM)] * 12,
            out_specs=pl.BlockSpec(memory_space=pltpu.VMEM),
            scratch_shapes=scratch,
            compiler_params=pltpu.CompilerParams(
                collective_id=0, has_side_effects=True, vmem_limit_bytes=60 * 1024 * 1024
            ),
        )(*arrays)

    return jax.shard_map(
        local,
        mesh=mesh,
        in_specs=(
            P(("grp", "fs"), None),
            P(),
            P("fs", "tp"),
            P("fs", "tp"),
            P("fs", "tp"),
            P("tp"),
            P("tp"),
            P(),
            P(None, "tp"),
            P(None, "tp"),
            P("tp"),
            P("tp"),
        ),
        out_specs=P(("grp", "fs", "tp"), None),
        check_vma=False,
    )
```

time: 189 us -> 181 us (0.958)
  local copies, waits for them, and re-layouts: 7.05 us -> 1.88 us
  Pallas kernels: 181 us -> 178 us
    broadcast_in_dim x4 -> x0, local copies, waits for them, and re-layouts: 5.17 us -> none  [the longest x2 2.59 us: local(): scale[None]]
    pallas_call x1, Pallas kernels: 181 us -> 178 us  [local(): pl.pallas_call(functools.partial(kernel, parts, line, peers, pieces, lent...]
where the time goes in v2:
time: 181 us; the launch traced here: 180 us
  Pallas kernels  178 us (98%)
  local copies, waits for them, and re-layouts  1.88 us (1%)
    pallas_call x1, Pallas kernels, local(): pl.pallas_call(functools.partial(kernel, parts, line, peers, pieces, lent...  178 us

profile of v2, /device:TPU:0, one launch (start us, length us, event | category | flops | bytes accessed | tf_op | source)
XLA Modules:
  0.0 179.8 jit_solution(10234258952978355454)
XLA Ops:
  0.0 177.9 %shard_map.118 = bf16[128,2048]{1,0:T(8,128)(2,1)} custom-call(bf16[512,2048]{1,0:T(8,128)(2,1)} %tokens.1, f32[2048]{0:T(1024)} %norm_gain.1, f32[512,1408]{1,0:T(8,128)} %value_weight.1, f32[512,1408]{1,0:T(8,128)} %gate_weight.1, f32[512,1408]{1,0:T(8,128)} %down_weight.1, f32[1408]{0:T(1024)} %value_scale.1, f32[1408]{0:T(1024)} %gate_scale.1, ...), custom_call_target="tpu_custom_call" | custom-call | tf_op jit(solution)/shard_map/pallas_call | solution.py:477
  177.9 1.9 %copy.14 = bf16[128,2048]{1,0:T(8,128)(2,1)} copy(bf16[128,2048]{1,0:T(8,128)(2,1)} %shard_map.118) | data formatting | bytes 1048576

commit v3 on v2

--- a/solution.py
+++ b/solution.py
@@ -91,10 +91,12 @@
 
         lax.fori_loop(0, held // step, body, 0)
 
-    def copy(which, owner, part, slot, direction):
+    def copy(which, owner, part, slot, direction, neighbour=None):
         first = pl.multiple_of(owner * held + part * share + slot * piece, piece)
         block = full[which].at[pl.ds(first, piece), :]
-        if direction == RIGHT:
+        if neighbour is not None:
+            target = {"fs": neighbour}
+        elif direction == RIGHT:
             target = {"fs": lax.min(here + 1, line - 1)}
         elif direction == LEFT:
             target = {"fs": lax.max(here - 1, 0)}
@@ -125,6 +127,17 @@
                         lambda: act(copy(each, here, group, slot, direction))
                     )
 
+    def direct(each):
+        return bool(lent) and each != 3 * kinds - 1
+
+    def other(which, act):
+        for each in range(which, 3 * kinds, 3):
+            if direct(each):
+                for slot in range(pieces):
+                    for k in range(1, parts):
+                        part = lax.rem(group + k, parts)
+                        pl.when(end)(lambda: act(copy(each, here, part, slot, ACROSS + k - 1, mate)))
+
     def onward(which, step, act, arrive):
         for each in range(which, 3 * kinds, 3):
             for slot in range(pieces):
@@ -138,8 +151,15 @@
                         pl.when(more(each, direction))(
                             lambda: act(copy(each, owner, group, slot, direction))
                         )
-                        for k in range(parts - 1):
-                            act(copy(each, owner, group, slot, ACROSS + k))
+
+                        def share_out():
+                            for k in range(parts - 1):
+                                act(copy(each, owner, group, slot, ACROSS + k))
+
+                        if step == 1 and direct(each):
+                            pl.when(jnp.logical_and(owner > 0, owner < line - 1))(share_out)
+                        else:
+                            share_out()
 
     def crossed(which, step):
         for each in range(which, 3 * kinds, 3):
@@ -345,18 +365,26 @@
     ends = (here == 0).astype(jnp.int32) + (here == line - 1).astype(jnp.int32)
     pl.semaphore_wait(barrier, parts + peers - ends)
     own(0, start)
-    if lent:
-        pl.when(end)(lambda: lend().start())
     cast(1)
     own(1, start)
+    if lent:
+        pl.when(end)(lambda: lend().start())
+        other(0, start)
     cast(2)
+    if lent:
+        pl.when(end)(lambda: own(2, start))
+        other(1, start)
+        other(2, start)
     normalize(tokens, 0)
     for step in range(1, line):
         onward(0, step, start, True)
         if lent and step == 1:
             pl.when(helper)(relays)
     onward(1, 1, start, True)
-    own(2, start)
+    if lent:
+        pl.when(inner)(lambda: own(2, start))
+    else:
+        own(2, start)
     for step in range(1, line):
         crossed(0, step)
     value(0, mixed[0], 0)
@@ -425,6 +453,7 @@
     pltpu.make_async_copy(landed, landed, sum_send).wait()
     for which in range(3):
         own(which, left)
+        other(which, left)
         for step in range(1, line):
             onward(which, step, left, False)
 

time: 181 us -> 162 us (0.90)
  Pallas kernels: 178 us -> 160 us
    pallas_call x1, Pallas kernels: 178 us -> 160 us  [local(): pl.pallas_call(functools.partial(kernel, parts, line, peers, pieces, lent...]
where the time goes in v3:
time: 162 us
  Pallas kernels  160 us (99%)
  local copies, waits for them, and re-layouts  1.88 us (1%)
    pallas_call x1, Pallas kernels, local(): pl.pallas_call(functools.partial(kernel, parts, line, peers, pieces, lent...  160 us

profile of v3, /device:TPU:0, one launch (start us, length us, event | category | flops | bytes accessed | tf_op | source)
XLA Modules:
  0.0 161.7 jit_solution(17029206730685741683)
XLA Ops:
  0.0 159.8 %shard_map.118 = bf16[128,2048]{1,0:T(8,128)(2,1)} custom-call(bf16[512,2048]{1,0:T(8,128)(2,1)} %tokens.1, f32[2048]{0:T(1024)} %norm_gain.1, f32[512,1408]{1,0:T(8,128)} %value_weight.1, f32[512,1408]{1,0:T(8,128)} %gate_weight.1, f32[512,1408]{1,0:T(8,128)} %down_weight.1, f32[1408]{0:T(1024)} %value_scale.1, f32[1408]{0:T(1024)} %gate_scale.1, ...), custom_call_target="tpu_custom_call" | custom-call | tf_op jit(solution)/shard_map/pallas_call | solution.py:506
  159.9 1.9 %copy.14 = bf16[128,2048]{1,0:T(8,128)(2,1)} copy(bf16[128,2048]{1,0:T(8,128)(2,1)} %shard_map.118) | data formatting | bytes 1048576
